TPU v7x, 32 devices: a whole 2x2x4 slice. The times are simulated.
32 devices in a mesh: kv: 4 (over y, x), tp: 8 (over z, core).
Axes of the slice: x: 2, y: 2, z: 4, core: 2. Of those that a mesh axis runs over, the one named last changes fastest.
Arguments:
- stream: bfloat16 [32, 4096], P(None, ('kv', 'tp')), may hold values from -18 to 18
- mixer_gain: float32 [4096], replicated, may hold values from 0.1 to 1.9
- query_weight: bfloat16 [4096, 1024], P(None, 'tp'), may hold values from -0.09375 to 0.09375
- key_weight: bfloat16 [4096, 1024], P(None, 'tp'), may hold values from -0.09375 to 0.09375
- value_weight: bfloat16 [4096, 1024], P(None, 'tp'), may hold values from -0.09375 to 0.09375
- forget_weight: bfloat16 [4096, 16], replicated, may hold values from -0.09375 to 0.09375
- forget_bias: float32 [16], replicated, may hold values from -4 to -2
- key_cache: bfloat16 [32, 16, 4096, 64], P(None, 'tp', 'kv'), may hold values from -512 to 512, as said below
- value_cache: bfloat16 [32, 16, 4096, 64], P(None, 'tp', 'kv'), may hold values from -12 to 12
- past_decay: float32 [32, 16, 4096], P(None, 'tp', 'kv'), may hold values from -4096 to 0, as said below
- out_weight: bfloat16 [1024, 4096], P('tp', 'kv'), may hold values from -0.75 to 0.75
- channel_gain: float32 [4096], replicated, may hold values from 0.1 to 1.9
- up_weight: bfloat16 [4096, 16384], P('kv', 'tp'), may hold values from -0.09375 to 0.09375
- down_weight: bfloat16 [16384, 4096], P('tp', 'kv'), may hold values from -0.0625 to 0.0625
Outputs:
- updated: bfloat16 [32, 4096], P(None, ('kv', 'tp'))
Inputs may be any that keep to these rules, and one draw needn't show every extreme that they name: `key_cache`: keys of order one; some cached keys may be much larger. `past_decay`: never falling along the positions of a sequence and head, zero at the last cached position.
All inputs are finite; a program needn't handle non-finite values.
Results may differ from a plain program's by a relative error of at most 0.014.
The roundings to bfloat16 on the way count: a program that leaves them out, or rounds other values in their place, can miss the bound.
Values may be sent and summed in bfloat16 or wider, within the bound.
No kernel may reach another device: no remote copies, remote signals or barrier semaphores. Data moves between devices by JAX's collectives and lax.ppermute only.
A program may use at most 64 MiB of HBM per device.

v0:
```python
import jax
import jax.numpy as jnp
from jax import lax
from jax.sharding import PartitionSpec as P

D = 4096
EPS = 1e-06


def combined_all(part, axis, combine):
    gathered = jax.tree.map(lambda a: lax.all_gather(a, axis), part)

    def take(source):
        return jax.tree.map(lambda a: lax.dynamic_index_in_dim(a, source, 0, False), gathered)

    return lax.fori_loop(
        1, lax.axis_size(axis), lambda source, state: combine(state, take(source)), take(0)
    )


def rms_scale(values, gain):
    widened = values.astype(jnp.float32)
    inverse = lax.rsqrt(jnp.mean(widened * widened, axis=-1, keepdims=True) + EPS)
    return (widened * inverse * gain).astype(jnp.bfloat16)


def merge_parts(earlier, later):
    top_one, total_one, sums_one = earlier
    top_two, total_two, sums_two = later
    highest = jnp.maximum(top_one, top_two)
    factor_one = jnp.exp(top_one - highest)
    factor_two = jnp.exp(top_two - highest)
    return (
        highest,
        total_one * factor_one + total_two * factor_two,
        sums_one * factor_one[..., None] + sums_two * factor_two[..., None],
    )


def squared_relu(values):
    return jnp.square(jax.nn.relu(values)).astype(jnp.bfloat16)


def row_squares(values):
    widened = values.astype(jnp.float32)
    return jnp.sum(widened * widened, axis=1)


def shards(
    stream,
    mixer_gain,
    query_weight,
    key_weight,
    value_weight,
    forget_weight,
    forget_bias,
    key_cache,
    value_cache,
    past_decay,
    out_weight,
    channel_gain,
    up_weight,
    down_weight,
):
    batch_rows = stream.shape[0]
    local_heads = key_cache.shape[1]
    head_size = key_cache.shape[3]
    scale_factor = float(head_size) ** (-0.5)
    gathered = lax.all_gather(stream, ("kv", "tp"), axis=1, tiled=True)
    normed = rms_scale(gathered, mixer_gain)
    queries = jnp.dot(normed, query_weight, preferred_element_type=jnp.float32).astype(jnp.bfloat16)
    keys_new = jnp.dot(normed, key_weight, preferred_element_type=jnp.float32).astype(jnp.bfloat16)
    values_new = jnp.dot(normed, value_weight, preferred_element_type=jnp.float32).astype(
        jnp.bfloat16
    )
    forget_all = jax.nn.log_sigmoid(
        jnp.dot(normed, forget_weight, preferred_element_type=jnp.float32) + forget_bias
    )
    forget = lax.dynamic_slice_in_dim(
        forget_all, lax.axis_index("tp") * local_heads, local_heads, 1
    )
    query_heads = queries.reshape(batch_rows, local_heads, head_size)
    scores = (
        jnp.einsum("bhd,bhpd->bhp", query_heads, key_cache, preferred_element_type=jnp.float32)
        * scale_factor
        + forget[..., None]
        + past_decay
    )
    highest = jnp.max(scores, axis=-1)
    weights = jnp.exp(scores - highest[..., None]).astype(jnp.bfloat16)
    totals = jnp.sum(weights.astype(jnp.float32), axis=-1)
    sums = jnp.einsum("bhp,bhpd->bhd", weights, value_cache, preferred_element_type=jnp.float32)
    highest, totals, sums = combined_all((highest, totals, sums), "kv", merge_parts)
    key_heads = keys_new.reshape(batch_rows, local_heads, head_size).astype(jnp.float32)
    value_heads = values_new.reshape(batch_rows, local_heads, head_size).astype(jnp.float32)
    own = jnp.sum(query_heads.astype(jnp.float32) * key_heads, axis=-1) * scale_factor
    peak = jnp.maximum(highest, own)
    cache_factor = jnp.exp(highest - peak)
    own_factor = jnp.exp(own - peak)
    numer = sums * cache_factor[..., None] + value_heads * own_factor[..., None]
    denom = totals * cache_factor + own_factor
    attention = (
        (numer / denom[..., None]).astype(jnp.bfloat16).reshape(batch_rows, local_heads * head_size)
    )
    partial_value = jnp.dot(attention, out_weight, preferred_element_type=jnp.float32)
    piece_width = stream.shape[1]
    block_width = partial_value.shape[1]
    block_sum = lax.psum(partial_value, "tp")
    own_block = lax.dynamic_slice_in_dim(
        gathered, lax.axis_index("kv") * block_width, block_width, 1
    )
    middle_block = (own_block.astype(jnp.float32) + block_sum).astype(jnp.bfloat16)
    squares = lax.psum(row_squares(middle_block), "kv")
    middle_piece = lax.dynamic_slice_in_dim(
        middle_block, lax.axis_index("tp") * piece_width, piece_width, 1
    )
    inverse = lax.rsqrt(squares / D + EPS)
    gain_block = lax.dynamic_slice_in_dim(
        channel_gain, lax.axis_index("kv") * block_width, block_width, 0
    )
    mixed_block = (
        middle_block.astype(jnp.float32) * inverse[:, None] * gain_block[None, :]
    ).astype(jnp.bfloat16)
    up_partial = jnp.dot(mixed_block, up_weight, preferred_element_type=jnp.float32)
    hidden = squared_relu(lax.psum(up_partial, "kv"))
    down_partial = jnp.dot(hidden, down_weight, preferred_element_type=jnp.float32)
    reduced = lax.psum_scatter(down_partial, "tp", scatter_dimension=1, tiled=True)
    return (middle_piece.astype(jnp.float32) + reduced).astype(jnp.bfloat16)


def solution(mesh):
    return jax.shard_map(
        shards,
        mesh=mesh,
        in_specs=(
            P(None, ("kv", "tp")),
            P(),
            P(None, "tp"),
            P(None, "tp"),
            P(None, "tp"),
            P(),
            P(),
            P(None, "tp", "kv", None),
            P(None, "tp", "kv", None),
            P(None, "tp", "kv"),
            P("tp", "kv"),
            P(),
            P("kv", "tp"),
            P("tp", "kv"),
        ),
        out_specs=P(None, ("kv", "tp")),
        check_vma=False,
    )
```

profile of v0, /device:TPU:0, one launch (start us, length us, event | category | flops | bytes accessed | tf_op | source)
XLA Modules:
  0.0 247.9 jit_solution(13276194251928122677)
XLA Ops:
  6.5 44.6 %all_gather.21 = bf16[32,4096]{1,0:T(8,128)(2,1)S(1)} all-gather(bf16[32,128]{1,0:T(8,128)(2,1)} %param.16), channel_id=1, replica_groups=mesh['kv'=4,'tp'=8] {'kv','tp'}, dimensions={1}, use_global_device_ids=true | all-gather | bytes 270336 | tf_op jit(solution)/shard_map/all_gather | solution.py:69
  51.4 1.0 convolution_convert_fusion.2
  52.6 1.2 fusion.40
  53.9 4.6 %fusion.41 = f32[32,2,1,1024]{3,2,1,0:T(1,128)S(1)} fusion(bf16[32,2,64,1]{2,3,1,0:T(2,128)(2,1)S(1)} %reshape.57, bf16[32,2,1024,64]{2,3,1,0:T(8,128)(2,1)} %param.23), kind=kOutput, calls=%fused_computation.63 | convolution fusion | flops 8388608 | bytes 8658944 | tf_op jit(solution)/shard_map/bhd,bhpd->bhp/dot_general | solution.py:84
  58.5 2.1 fusion.38
  60.6 1.3 fusion.30
  61.9 5.7 %fusion.11 = f32[32,2,1,64]{3,2,1,0:T(1,128)S(1)} fusion(bf16[32,2,1024,64]{2,3,1,0:T(8,128)(2,1)} %param.24, bf16[32,2,1024,1]{2,1,0,3:T(2,128)(2,1)S(1)} %get-tuple-element.211), kind=kOutput, calls=%fused_computation.24 | convolution fusion | flops 8388608 | bytes 8536064 | tf_op jit(solution)/shard_map/bhp,bhpd->bhd/dot_general | solution.py:92
  67.6 7.5 %all-gather.2 = f32[128,2,64]{2,1,0:T(2,128)S(1)} all-gather(f32[32,2,64]{2,1,0:T(2,128)S(1)} %bitcast.49), channel_id=4, replica_groups=mesh['kv'=4,'tp'=8] {'kv'}, dimensions={0}, use_global_device_ids=true | all-gather | bytes 81920 | tf_op jit(solution)/shard_map/all_gather | solution.py:11
  75.8 8.1 %all-gather.4 = f32[4,32,2]{1,2,0:T(2,128)S(1)} all-gather(f32[1,32,2]{1,2,0:T(2,128)S(1)} %bitcast.51), channel_id=3, replica_groups=mesh['kv'=4,'tp'=8] {'kv'}, dimensions={0}, use_global_device_ids=true | all-gather | bytes 1280 | tf_op jit(solution)/shard_map/all_gather | solution.py:11
  83.8 7.1 %all-gather.3 = f32[4,32,2]{1,2,0:T(2,128)S(1)} all-gather(f32[1,32,2]{1,2,0:T(2,128)S(1)} %bitcast.50), channel_id=2, replica_groups=mesh['kv'=4,'tp'=8] {'kv'}, dimensions={0}, use_global_device_ids=true | all-gather | bytes 1280 | tf_op jit(solution)/shard_map/all_gather | solution.py:11
  90.9 3.6 %while.19 = (s32[]{:T(128)}, f32[32,2]{0,1:T(2,128)S(1)}, f32[32,2]{0,1:T(2,128)S(1)}, f32[32,2,64]{2,1,0:T(2,128)S(1)}, f32[4,32,2]{1,2,0:T(2,128)S(1)}, /*inde...) while((s32[]{:T(128)}, f32[32,2]{0,1:T(2,128)S(1)}, ...), condition=%wide.region_4.5_spmd, body=%wide.region_3.4_spmd.sunk | while | flops 12677 | bytes 52887 | solution.py:16
  91.1 1.0 fusion.57
  92.3 1.0 fusion.57
  93.5 1.0 fusion.57
  96.2 1.8 fusion.42
  98.0 0.7 dynamic_slice.59
  98.7 51.7 %all-reduce.3.cloned.1.call-done = f32[32,1024]{1,0:T(8,128)} async-done(((f32[32,1024]{1,0:T(8,128)}), f32[32,1024]{1,0:T(8,128)}) %all-reduce.3.cloned.1.call-update) | async-done | bytes 131088 | tf_op jit(solution)/shard_map/psum | solution.py:108
  150.4 1.0 fusion.13
  151.4 9.8 %psum.22 = f32[32]{0:T(128)S(1)} all-reduce(f32[32]{0:T(128)S(1)} %get-tuple-element.204), channel_id=1, replica_groups=mesh['kv'=4,'tp'=8] {'kv'}, use_global_device_ids=true, to_apply=%region_8.9 | all-reduce | flops 32 | bytes 256 | tf_op jit(solution)/shard_map/psum | solution.py:113
  161.3 3.8 %fusion.18 = f32[32,2048]{1,0:T(8,128)} fusion(bf16[1024,2048]{1,0:T(8,128)(2,1)} %param.28, bf16[32,1024]{1,0:T(8,128)(2,1)S(1)} %get-tuple-element.205, f32[1024]{0:T(1024)S(1)} %dynamic_slice.59, f32[32]{0:T(128)S(1)} %add_rsqrt_fusion), kind=kOutput, calls=%fused_computation.37 | convolution fusion | flops 134348800 | bytes 4526208 | tf_op jit(solution)/shard_map/dot_general | solution.py:124
  165.1 40.4 %all-reduce.5.cloned.1.call-done = f32[32,2048]{1,0:T(8,128)} async-done(((f32[32,2048]{1,0:T(8,128)}), f32[32,2048]{1,0:T(8,128)}) %all-reduce.5.cloned.1.call-update) | async-done | bytes 262160 | tf_op jit(solution)/shard_map/psum | solution.py:125
  205.5 3.8 %fusion.16 = f32[32,1024]{1,0:T(8,128)} fusion(bf16[2048,1024]{1,0:T(8,128)(2,1)} %param.29, f32[32,2048]{1,0:T(8,128)} %all-reduce.5.cloned.1.call-done), kind=kOutput, calls=%fused_computation.34 | convolution fusion | flops 134414336 | bytes 4587520 | tf_op jit(solution)/shard_map/dot_general | solution.py:126
  209.3 30.7 %reduce-scatter.2.cloned.1.call-done = f32[32,128]{1,0:T(8,128)} async-done(((f32[32,1024]{1,0:T(8,128)}), f32[32,128]{1,0:T(8,128)}) %reduce-scatter.2.cloned.1.call-update) | async-done | bytes 16400 | tf_op jit(solution)/shard_map/reduce_scatter | solution.py:127
  240.0 1.3 add_convert_fusion.1
  (49 shorter events, 3.6 us)
Async XLA Ops:
  6.5 44.8 %copy-start = (bf16[4096,128]{1,0:T(8,128)(2,1)S(1)}, bf16[4096,128]{1,0:T(8,128)(2,1)}, u32[]{:S(2)}) copy-start(bf16[4096,128]{1,0:T(8,128)(2,1)} %param.18) | copy-start | bytes 3145732
  6.5 143.8 %all-reduce.3.cloned.1.call-start = ((), (), s32[]{:S(2)}) async-start(), calls=%async_computation.1 | async-start | bytes 262144 | tf_op jit(solution)/shard_map/psum | solution.py:108
  58.4 36.1 %copy-start.1 = (bf16[4096,128]{1,0:T(8,128)(2,1)S(1)}, bf16[4096,128]{1,0:T(8,128)(2,1)}, u32[]{:S(2)}) copy-start(bf16[4096,128]{1,0:T(8,128)(2,1)} %param.19) | copy-start | bytes 3145732
  58.4 36.1 %copy-start.4 = (f32[4096]{0:T(1024)S(1)}, f32[4096]{0:T(1024)}, u32[]{:S(2)}) copy-start(f32[4096]{0:T(1024)} %param.17) | copy-start | bytes 49156
  58.5 37.0 %copy-start.2 = (bf16[4096,128]{1,0:T(8,128)(2,1)S(1)}, bf16[4096,128]{1,0:T(8,128)(2,1)}, u32[]{:S(2)}) copy-start(bf16[4096,128]{1,0:T(8,128)(2,1)} %param.20) | copy-start | bytes 3145732
  75.0 0.6 copy-start.3
  98.0 107.5 %all-reduce.5.cloned.1.call-start = ((), (), s32[]{:S(2)}) async-start(), calls=%async_computation.2 | async-start | bytes 524288 | tf_op jit(solution)/shard_map/psum | solution.py:125
  165.1 75.0 %reduce-scatter.2.cloned.1.call-start = ((), (), s32[]{:S(2)}) async-start(), calls=%async_computation.3 | async-start | bytes 147456 | tf_op jit(solution)/shard_map/reduce_scatter | solution.py:127
Sparse Core Ops, SparseCore 0:
  98.1 52.2 all-reduce.2
  165.2 40.2 all-reduce.4
  209.4 30.5 reduce-scatter.1
where the time goes:
time: 249 us; the launch traced here: 248 us
  waiting for transfers between devices  123 us (49%)
  blocking collectives  77.1 us (31%)
  matrix products  22.4 us (9%)
  between operations  13.2 us (5%)
  other arithmetic  9.28 us (4%)
  local copies, waits for them, and re-layouts  2.9 us (1%)
    psum x1, waiting for transfers between devices, shards(): block_sum = lax.psum(partial_value, 'tp')  51.7 us
    all_gather x1, blocking collectives, shards(): gathered = lax.all_gather(stream, ('kv', 'tp'), axis=1, tiled=True)  44.6 us
    psum x1, waiting for transfers between devices, shards(): hidden = squared_relu(lax.psum(up_partial, 'kv'))  40.4 us
    reduce_scatter x1, waiting for transfers between devices, shards(): lax.psum_scatter(down_partial, 'tp', scatter_dimension=1, tiled=True)  30.7 us
    all_gather x3, blocking collectives, combined_all(): gathered = jax.tree.map(lambda a: lax.all_gather(a, axis), part)  22.6 us
    psum x1, blocking collectives, shards(): squares = lax.psum(row_squares(middle_block), 'kv')  9.84 us
    dot_general x1, matrix products, shards(): jnp.einsum('bhp,bhpd->bhd', weights, value_cache, preferred_element_type=...  5.65 us
  transfers between devices with their start and end apart: 3, of which 3 were waited for; matrix products, arithmetic and copies ran while one was open for 0% of the time, Pallas kernels for 0%

commit v1 on v0

--- a/solution.py
+++ b/solution.py
@@ -105,7 +105,7 @@
     partial_value = jnp.dot(attention, out_weight, preferred_element_type=jnp.float32)
     piece_width = stream.shape[1]
     block_width = partial_value.shape[1]
-    block_sum = lax.psum(partial_value, "tp")
+    block_sum = jnp.sum(lax.all_gather(partial_value, "tp"), axis=0)
     own_block = lax.dynamic_slice_in_dim(
         gathered, lax.axis_index("kv") * block_width, block_width, 1
     )

time: 249 us -> 217 us (0.87)
  waiting for transfers between devices: 123 us -> 90.7 us
    psum x1 -> x0, waiting for transfers between devices: 51.7 us -> none  [shards(): block_sum = lax.psum(partial_value, 'tp')]
    all_gather x0 -> x1, waiting for transfers between devices: none -> 18.9 us  [shards(): block_sum = jnp.sum(lax.all_gather(partial_value, 'tp'), axis=0)]
where the time goes in v1:
time: 217 us; the launch traced here: 216 us
  waiting for transfers between devices  90.7 us (42%)
  blocking collectives  77.1 us (36%)
  matrix products  22.4 us (10%)
  between operations  13.2 us (6%)
  other arithmetic  9.68 us (4%)
  local copies, waits for them, and re-layouts  2.9 us (1%)
    all_gather x1, blocking collectives, shards(): gathered = lax.all_gather(stream, ('kv', 'tp'), axis=1, tiled=True)  44.6 us
    psum x1, waiting for transfers between devices, shards(): hidden = squared_relu(lax.psum(up_partial, 'kv'))  40.9 us
    reduce_scatter x1, waiting for transfers between devices, shards(): lax.psum_scatter(down_partial, 'tp', scatter_dimension=1, tiled=True)  30.7 us
    all_gather x3, blocking collectives, combined_all(): gathered = jax.tree.map(lambda a: lax.all_gather(a, axis), part)  22.6 us
    all_gather x1, waiting for transfers between devices, shards(): block_sum = jnp.sum(lax.all_gather(partial_value, 'tp'), axis=0)  18.9 us
    psum x1, blocking collectives, shards(): squares = lax.psum(row_squares(middle_block), 'kv')  9.83 us
    dot_general x1, matrix products, shards(): jnp.einsum('bhp,bhpd->bhd', weights, value_cache, preferred_element_type=...  5.65 us
    dot_general x1, matrix products, shards(): jnp.einsum('bhd,bhpd->bhp', query_heads, key_cache, preferred_element_typ...  4.59 us
  transfers between devices with their start and end apart: 3, of which 3 were waited for; matrix products, arithmetic and copies ran while one was open for 0% of the time, Pallas kernels for 0%

profile of v1, /device:TPU:0, one launch (start us, length us, event | category | flops | bytes accessed | tf_op | source)
XLA Modules:
  0.0 216.1 jit_solution(4532986432456008099)
XLA Ops:
  6.5 44.6 %all_gather.27 = bf16[32,4096]{1,0:T(8,128)(2,1)S(1)} all-gather(bf16[32,128]{1,0:T(8,128)(2,1)} %param.16), channel_id=1, replica_groups=mesh['kv'=4,'tp'=8] {'kv','tp'}, dimensions={1}, use_global_device_ids=true | all-gather | bytes 270336 | tf_op jit(solution)/shard_map/all_gather | solution.py:69
  51.4 1.0 convolution_convert_fusion.2
  52.6 1.2 fusion.40
  53.9 4.6 %fusion.41 = f32[32,2,1,1024]{3,2,1,0:T(1,128)S(1)} fusion(bf16[32,2,64,1]{2,3,1,0:T(2,128)(2,1)S(1)} %reshape.58, bf16[32,2,1024,64]{2,3,1,0:T(8,128)(2,1)} %param.23), kind=kOutput, calls=%fused_computation.63 | convolution fusion | flops 8388608 | bytes 8658944 | tf_op jit(solution)/shard_map/bhd,bhpd->bhp/dot_general | solution.py:84
  58.5 2.1 fusion.38
  60.6 1.3 fusion.30
  61.9 5.7 %fusion.11 = f32[32,2,1,64]{3,2,1,0:T(1,128)S(1)} fusion(bf16[32,2,1024,64]{2,3,1,0:T(8,128)(2,1)} %param.24, bf16[32,2,1024,1]{2,1,0,3:T(2,128)(2,1)S(1)} %get-tuple-element.211), kind=kOutput, calls=%fused_computation.24 | convolution fusion | flops 8388608 | bytes 8536064 | tf_op jit(solution)/shard_map/bhp,bhpd->bhd/dot_general | solution.py:92
  67.6 7.5 %all-gather.2 = f32[128,2,64]{2,1,0:T(2,128)S(1)} all-gather(f32[32,2,64]{2,1,0:T(2,128)S(1)} %bitcast.51), channel_id=4, replica_groups=mesh['kv'=4,'tp'=8] {'kv'}, dimensions={0}, use_global_device_ids=true | all-gather | bytes 81920 | tf_op jit(solution)/shard_map/all_gather | solution.py:11
  75.8 8.1 %all-gather.5 = f32[4,32,2]{1,2,0:T(2,128)S(1)} all-gather(f32[1,32,2]{1,2,0:T(2,128)S(1)} %bitcast.53), channel_id=3, replica_groups=mesh['kv'=4,'tp'=8] {'kv'}, dimensions={0}, use_global_device_ids=true | all-gather | bytes 1280 | tf_op jit(solution)/shard_map/all_gather | solution.py:11
  83.8 7.1 %all-gather.4 = f32[4,32,2]{1,2,0:T(2,128)S(1)} all-gather(f32[1,32,2]{1,2,0:T(2,128)S(1)} %bitcast.52), channel_id=2, replica_groups=mesh['kv'=4,'tp'=8] {'kv'}, dimensions={0}, use_global_device_ids=true | all-gather | bytes 1280 | tf_op jit(solution)/shard_map/all_gather | solution.py:11
  90.9 3.6 %while.19 = (s32[]{:T(128)}, f32[32,2]{0,1:T(2,128)S(1)}, f32[32,2]{0,1:T(2,128)S(1)}, f32[32,2,64]{2,1,0:T(2,128)S(1)}, f32[4,32,2]{1,2,0:T(2,128)S(1)}, /*inde...) while((s32[]{:T(128)}, f32[32,2]{0,1:T(2,128)S(1)}, ...), condition=%wide.region_4.5_spmd, body=%wide.region_3.4_spmd.sunk | while | flops 12677 | bytes 52887 | solution.py:16
  91.1 1.0 fusion.57
  92.3 1.0 fusion.57
  93.5 1.0 fusion.57
  96.2 1.8 fusion.42
  98.0 0.7 dynamic_slice.59
  98.7 18.9 %all-gather.8.cloned.1.call-done = f32[256,1024]{1,0:T(8,128)} async-done(((f32[32,1024]{1,0:T(8,128)}), f32[256,1024]{1,0:T(8,128)}) %all-gather.8.cloned.1.call-update) | async-done | bytes 1048592 | tf_op jit(solution)/shard_map/all_gather | solution.py:108
  117.6 1.3 reduce_sum.48
  119.1 9.8 %psum.14 = f32[32]{0:T(128)S(1)} all-reduce(f32[32]{0:T(128)S(1)} %get-tuple-element.204), channel_id=1, replica_groups=mesh['kv'=4,'tp'=8] {'kv'}, use_global_device_ids=true, to_apply=%region_8.9 | all-reduce | flops 32 | bytes 256 | tf_op jit(solution)/shard_map/psum | solution.py:113
  128.9 3.8 %fusion.18 = f32[32,2048]{1,0:T(8,128)} fusion(bf16[1024,2048]{1,0:T(8,128)(2,1)} %param.28, bf16[32,1024]{1,0:T(8,128)(2,1)S(1)} %get-tuple-element.205, f32[1024]{0:T(1024)S(1)} %dynamic_slice.59, f32[32]{0:T(128)S(1)} %add_rsqrt_fusion), kind=kOutput, calls=%fused_computation.37 | convolution fusion | flops 134348800 | bytes 4526208 | tf_op jit(solution)/shard_map/dot_general | solution.py:124
  132.8 40.9 %all-reduce.2.cloned.1.call-done = f32[32,2048]{1,0:T(8,128)} async-done(((f32[32,2048]{1,0:T(8,128)}), f32[32,2048]{1,0:T(8,128)}) %all-reduce.2.cloned.1.call-update) | async-done | bytes 262160 | tf_op jit(solution)/shard_map/psum | solution.py:125
  173.7 3.8 %fusion.16 = f32[32,1024]{1,0:T(8,128)} fusion(bf16[2048,1024]{1,0:T(8,128)(2,1)} %param.29, f32[32,2048]{1,0:T(8,128)} %all-reduce.2.cloned.1.call-done), kind=kOutput, calls=%fused_computation.34 | convolution fusion | flops 134414336 | bytes 4587520 | tf_op jit(solution)/shard_map/dot_general | solution.py:126
  177.5 30.7 %reduce-scatter.2.cloned.1.call-done = f32[32,128]{1,0:T(8,128)} async-done(((f32[32,1024]{1,0:T(8,128)}), f32[32,128]{1,0:T(8,128)}) %reduce-scatter.2.cloned.1.call-update) | async-done | bytes 16400 | tf_op jit(solution)/shard_map/reduce_scatter | solution.py:127
  208.2 1.3 add_convert_fusion.1
  (50 shorter events, 3.7 us)
Async XLA Ops:
  6.5 44.8 %copy-start = (bf16[4096,128]{1,0:T(8,128)(2,1)S(1)}, bf16[4096,128]{1,0:T(8,128)(2,1)}, u32[]{:S(2)}) copy-start(bf16[4096,128]{1,0:T(8,128)(2,1)} %param.18) | copy-start | bytes 3145732
  6.5 111.1 %all-gather.8.cloned.1.call-start = ((), (), s32[]{:S(2)}) async-start(), calls=%async_computation.3 | async-start | bytes 1179648 | tf_op jit(solution)/shard_map/all_gather | solution.py:108
  58.4 36.1 %copy-start.1 = (bf16[4096,128]{1,0:T(8,128)(2,1)S(1)}, bf16[4096,128]{1,0:T(8,128)(2,1)}, u32[]{:S(2)}) copy-start(bf16[4096,128]{1,0:T(8,128)(2,1)} %param.19) | copy-start | bytes 3145732
  58.4 36.1 %copy-start.4 = (f32[4096]{0:T(1024)S(1)}, f32[4096]{0:T(1024)}, u32[]{:S(2)}) copy-start(f32[4096]{0:T(1024)} %param.17) | copy-start | bytes 49156
  58.5 37.0 %copy-start.2 = (bf16[4096,128]{1,0:T(8,128)(2,1)S(1)}, bf16[4096,128]{1,0:T(8,128)(2,1)}, u32[]{:S(2)}) copy-start(bf16[4096,128]{1,0:T(8,128)(2,1)} %param.20) | copy-start | bytes 3145732
  75.0 0.6 copy-start.3
  98.0 75.7 %all-reduce.2.cloned.1.call-start = ((), (), s32[]{:S(2)}) async-start(), calls=%async_computation.1 | async-start | bytes 524288 | tf_op jit(solution)/shard_map/psum | solution.py:125
  132.7 75.5 %reduce-scatter.2.cloned.1.call-start = ((), (), s32[]{:S(2)}) async-start(), calls=%async_computation.2 | async-start | bytes 147456 | tf_op jit(solution)/shard_map/reduce_scatter | solution.py:127
Sparse Core Ops, SparseCore 0:
  98.1 19.5 all-gather.7
  132.8 40.8 all-reduce.1
  177.6 30.5 reduce-scatter.1
